TPU v7x, 32 devices: a whole 2x2x4 slice. The times are simulated.
32 devices in a mesh: ep: 8 (over z, x), tp: 4 (over y, core).
Axes of the slice: x: 2, y: 2, z: 4, core: 2. Of those that a mesh axis runs over, the one named last changes fastest.
Arguments:
- out_gate: bfloat16 [8192, 1024], P('ep', 'tp'), may hold values from -6 to 6
- in_gate: bfloat16 [8192, 1024], P('ep', 'tp'), may hold values from -6 to 6
- conv_input: bfloat16 [8192, 1024], P('ep', 'tp'), may hold values from -6 to 6
- conv_taps: float32 [3, 1024], P(None, 'tp'), may hold values from -4 to 4
- group_gain: float32 [1024], P('tp'), may hold values from 0.1 to 1.9
- mix_out_w: bfloat16 [1024, 2048], replicated, may hold values from -0.1875 to 0.1875
- moe_in: bfloat16 [8192, 2048], P(('ep', 'tp')), may hold values from -6 to 6
- moe_gain: float32 [2048], replicated, may hold values from 0.1 to 1.9
- route_ids: int32 [8192, 2], P(('ep', 'tp')), may hold values from 0 to 31, as said below
- route_weight: float32 [8192, 2], P(('ep', 'tp')), may hold values from 0.1 to 1
- gate_w: bfloat16 [32, 2048, 1024], P(('ep', 'tp')), may hold values from -0.125 to 0.125
- up_w: bfloat16 [32, 2048, 1024], P(('ep', 'tp')), may hold values from -0.125 to 0.125
- down_w: bfloat16 [32, 1024, 2048], P(('ep', 'tp')), may hold values from -0.1875 to 0.1875
Outputs:
- mixed: bfloat16 [8192, 2048], P(('ep', 'tp'))
- moe_out: bfloat16 [8192, 2048], P(('ep', 'tp'))
Inputs may be any that keep to these rules, and one draw needn't show every extreme that they name: `route_ids`: the two numbers of a row are different experts of one group: group g holds experts g * 4 to g * 4 + 3. The rows of one device (aligned blocks of 256 rows) name each group in exactly 32 rows and each expert in exactly 16 rows.
All inputs are finite; a program needn't handle non-finite values.
Results may differ from a plain program's by a relative error of at most 0.0071.
Values may be sent and summed in bfloat16 or wider, within the bound.
A program may use at most 128 MiB of HBM per device.

v0:
```python
import jax
import jax.numpy as jnp
from jax import lax
from jax.sharding import PartitionSpec as P

GROUP_CH = 64


def shifted(value, axis, by):
    count = lax.axis_size(axis)
    pairs = [(i, i + by) for i in range(count) if 0 <= i + by < count]
    return lax.ppermute(value, axis, pairs)


def expert_rows(inputs, w_gate, w_up, w_down):
    gate_part = jnp.dot(inputs, w_gate, preferred_element_type=jnp.float32)
    up_part = jnp.dot(inputs, w_up, preferred_element_type=jnp.float32)
    hidden = (jax.nn.silu(gate_part) * up_part).astype(jnp.bfloat16)
    return jnp.dot(hidden, w_down, preferred_element_type=jnp.float32).astype(jnp.bfloat16)


def place_ranks(labels_in, bins, per_bin):
    hits = (labels_in[:, None] == jnp.arange(bins, dtype=jnp.int32)[None, :]).astype(jnp.int32)
    before = jnp.cumsum(hits, axis=0) - hits
    return labels_in * per_bin + jnp.sum(before * hits, axis=1)


def shards(
    out_gate,
    in_gate,
    conv_input,
    conv_taps,
    group_gain,
    mix_out_w,
    moe_in,
    moe_gain,
    route_ids,
    route_weight,
    gate_w,
    up_w,
    down_w,
):
    rows_ep, channels = in_gate.shape
    member_count = lax.axis_size("tp")
    group_count = lax.axis_size("ep")
    reach = conv_taps.shape[0] - 1
    edge_rows = jnp.stack([in_gate[rows_ep - reach :], conv_input[rows_ep - reach :]])
    earlier = shifted(edge_rows, "ep", 1)
    product = in_gate.astype(jnp.float32) * conv_input.astype(jnp.float32)
    before_rows = earlier[0].astype(jnp.float32) * earlier[1].astype(jnp.float32)
    padded = jnp.concatenate([before_rows, product], axis=0)
    convolved = jnp.zeros_like(product)
    for tap in range(reach + 1):
        convolved = convolved + conv_taps[tap] * padded[tap : tap + rows_ep]
    gated = out_gate.astype(jnp.float32) * convolved
    grouped = gated.reshape(rows_ep, channels // GROUP_CH, GROUP_CH)
    inv_rms = lax.rsqrt(jnp.mean(grouped * grouped, axis=-1, keepdims=True) + 1e-06)
    normed = ((grouped * inv_rms).reshape(rows_ep, channels) * group_gain).astype(jnp.bfloat16)
    blocks = normed.reshape(member_count, rows_ep // member_count, channels)
    portion = lax.all_to_all(blocks, "tp", split_axis=0, concat_axis=2, tiled=True)
    flat_rows = portion.reshape(-1, portion.shape[2])
    projected = jnp.dot(flat_rows, mix_out_w, preferred_element_type=jnp.float32).astype(
        jnp.bfloat16
    )
    mixed = projected.reshape(portion.shape[0], portion.shape[1], -1)
    mixed = mixed.reshape(-1, mixed.shape[2])
    tok_count, width = moe_in.shape
    wide_in = moe_in.astype(jnp.float32)
    rms_scale = lax.rsqrt(jnp.mean(wide_in * wide_in, axis=-1, keepdims=True) + 1e-06)
    expert_in = (wide_in * rms_scale * moe_gain).astype(jnp.bfloat16)
    w_gate = gate_w[0]
    w_up = up_w[0]
    w_down = down_w[0]
    expert_count = group_count * member_count
    slot_count = 2 * tok_count // expert_count
    flat_ids = route_ids.reshape(-1)
    target = place_ranks(flat_ids, expert_count, slot_count)
    owners = jnp.arange(2 * tok_count, dtype=jnp.int32) // 2
    sources = jnp.zeros((expert_count * slot_count,), jnp.int32).at[target].set(owners)
    outgoing = expert_in[sources].reshape(expert_count, slot_count, width)
    portion = lax.all_to_all(outgoing, ("ep", "tp"), split_axis=0, concat_axis=0, tiled=True)
    sources, amount, _ = portion.shape
    returned = lax.all_to_all(
        expert_rows(portion.reshape(-1, width), w_gate, w_up, w_down).reshape(
            sources, amount, width
        ),
        ("ep", "tp"),
        split_axis=0,
        concat_axis=0,
        tiled=True,
    )
    results = returned.reshape(-1, width)[target].reshape(tok_count, 2, width)
    first_out = results[:, 0].astype(jnp.float32)
    second = results[:, 1].astype(jnp.float32)
    moe_out = (first_out * route_weight[:, 0:1] + second * route_weight[:, 1:2]).astype(
        jnp.bfloat16
    )
    return (mixed, moe_out)


def solution(mesh):
    in_specs = (
        P("ep", "tp"),
        P("ep", "tp"),
        P("ep", "tp"),
        P(None, "tp"),
        P("tp"),
        P(),
        P(("ep", "tp"), None),
        P(),
        P(("ep", "tp"), None),
        P(("ep", "tp"), None),
        P(("ep", "tp"), None, None),
        P(("ep", "tp"), None, None),
        P(("ep", "tp"), None, None),
    )
    out_specs = (P(("ep", "tp"), None), P(("ep", "tp"), None))
    return jax.shard_map(shards, mesh=mesh, in_specs=in_specs, out_specs=out_specs, check_vma=False)
```

profile of v0, /device:TPU:0, one launch (start us, length us, event | category | flops | bytes accessed | tf_op | source)
XLA Modules:
  0.0 157.8 jit_solution(7375254399032966453)
XLA Ops:
  0.6 0.0 copy-start
  0.6 0.0 copy-start.3
  0.7 0.9 copy.35
  1.6 0.1 eq.29
  1.7 0.1 eq.25
  1.8 0.7 broadcast_multiply_fusion
  2.5 1.2 reduce-window.6
  3.7 0.2 slice_reduce_fusion
  4.0 0.1 copy.34
  4.1 0.1 mul.159
  4.3 0.1 fusion.28
  4.4 2.4 %scatter_custom_fusion = s32[512]{0:T(512)S(1)} fusion(s32[512]{0:T(512)S(1)} %bitcast.88, s32[512]{0:T(512)S(1)} %add_select_fusion, s32[]{:T(128)} %constant.35.clone.1), kind=kCustom, calls=%fused_computation.62 | custom fusion | bytes 2052 | tf_op jit(solution)/shard_map/scatter | solution.py:79
  6.9 1.5 fusion.9
  8.4 0.0 copy-done
  8.4 0.0 copy-done.3
  8.4 0.3 fusion.11
  8.7 3.3 %gather_fusion = bf16[512,2048]{1,0:T(8,128)(2,1)} fusion(bf16[256,2048]{1,0:T(8,128)(2,1)S(1)} %fusion.11, s32[1024]{0:T(1024)S(1)} %pad_clamp_fusion.1), kind=kCustom, calls=%fused_computation | custom fusion | bytes 4196352 | tf_op jit(solution)/shard_map/gather | solution.py:80
  12.1 0.0 copy-start.1
  12.1 7.3 %all-to-all-start.1 = ((bf16[32,16,2048]{2,1,0:T(8,128)(2,1)}), bf16[32,16,2048]{2,1,0:T(8,128)(2,1)S(1)}, u32[]{:S(2)}, u32[]{:S(2)}) async-start(bf16[32,16,2048]{2,1,0:T(8,128)(2,1)} %bitcast.14), calls=%async_computation.1 | async-start | bytes 4194304 | tf_op jit(solution)/shard_map/all_to_all | solution.py:81
  19.4 0.0 copy-done.1
  19.4 0.0 copy-done.2
  19.5 0.2 copy.30
  19.6 0.0 copy-start.4
  19.7 3.7 %collective-permute-start = (bf16[2,2,256]{1,2,0:T(8,128)(2,1)S(1)}, bf16[2,2,256]{1,2,0:T(8,128)(2,1)S(1)}, u32[]{:S(2)}, u32[]{:S(2)}) collective-permute-start(bf16[2,2,256]{1,2,0:T(8,128)(2,1)S(1)} %copy.30), channel_id=1, source_target_pairs={{0,4},{4,8},{8,12},{12,16},{16,20},{20,24},{24,28},{1,5},{5,9},{9,... | collective-permute-start | bytes 6152 | tf_op jit(solution)/shard_map/ppermute | solution.py:12
  23.3 1.0 copy.31
  24.3 1.0 copy.32
  25.3 1.4 convert_multiply_fusion.4
  26.7 0.0 copy-done.4
  26.7 0.0 copy-start.6
  26.8 2.0 %copy.29 = bf16[1024,256]{0,1:T(8,128)(2,1)} copy(bf16[1024,256]{1,0:T(8,128)(2,1)} %param.13) | data formatting | bytes 1048576 | tf_op args[0]
  28.8 11.3 %collective-permute-done = bf16[2,2,256]{1,2,0:T(8,128)(2,1)S(1)} collective-permute-done((bf16[2,2,256]{1,2,0:T(8,128)(2,1)S(1)}, bf16[2,2,256]{1,2,0:T(8,128)(2,1)S(1)}, u32[]{:S(2)}, u32[]{:S(2)}) %collective-permute-start) | collective-permute-done | bytes 2080 | tf_op jit(solution)/shard_map/ppermute | solution.py:12
  40.1 1.8 %bitcast_reduce_fusion = (f32[1024,4]{0,1:T(4,128)S(1)}, f32[1024,256]{0,1:T(8,128)S(1)}) fusion(f32[1024,256]{0,1:T(8,128)S(1)} %convert_multiply_fusion.4, f32[256]{0:T(256)S(1)} %bitcast.94, f32[2,256]{0,1:T(8,128)S(1)} %multiply_bitcast_fusion, f32[256]{0:T(256)S(1)} %bitcast.95, f32[256]{0:T(256)S(1)} %bitcast.93, bf16[1024,256]{0,1:T(8,128)(2,1)} %copy.29), kind=kLoop, calls=%fused_computation.35 | loop fusion | flops 2879488 | bytes 2642944 | tf_op jit(solution)/shard_map/reduce_sum | solution.py:57
  42.0 0.0 copy-done.6
  42.0 0.2 fusion.23
  42.2 0.8 copy.52
  43.0 25.1 %all-to-all-done.1 = bf16[32,16,2048]{2,1,0:T(8,128)(2,1)S(1)} async-done(((bf16[32,16,2048]{2,1,0:T(8,128)(2,1)}), bf16[32,16,2048]{2,1,0:T(8,128)(2,1)S(1)}, u32[]{:S(2)}, u32[]{:S(2)}) %all-to-all-start.1) | async-done | bytes 2097184 | tf_op jit(solution)/shard_map/all_to_all | solution.py:81
  68.1 3.5 %all-to-all-start = ((bf16[4,256,256]{1,2,0:T(8,128)(2,1)}), bf16[4,256,256]{1,2,0:T(8,128)(2,1)S(1)}, u32[]{:S(2)}, u32[]{:S(2)}) async-start(bf16[4,256,256]{1,2,0:T(8,128)(2,1)} %bitcast.81), calls=%async_computation | async-start | bytes 1048576 | tf_op jit(solution)/shard_map/all_to_all | solution.py:60
  71.6 5.9 %fusion.4 = f32[512,1024]{1,0:T(8,128)} fusion(bf16[512,2048]{1,0:T(8,128)(2,1)S(1)} %bitcast.83, bf16[1,2048,1024]{2,1,0:T(8,128)(2,1)} %param.23), kind=kOutput, calls=%fused_computation.7 | convolution fusion | flops 2147483648 | bytes 8388608 | tf_op jit(solution)/shard_map/dot_general | solution.py:16
  77.5 9.9 %fusion.6 = bf16[512,2048]{1,0:T(8,128)(2,1)} fusion(bf16[1,1024,2048]{2,1,0:T(8,128)(2,1)} %param.25, f32[512,1024]{1,0:T(8,128)} %fusion.4, bf16[512,2048]{1,0:T(8,128)(2,1)S(1)} %bitcast.84, bf16[1,2048,1024]{2,1,0:T(8,128)(2,1)} %param.24), kind=kOutput, calls=%fused_computation.9 | convolution fusion | flops 4299161600 | bytes 14680064 | tf_op jit(solution)/shard_map/dot_general | solution.py:19
  87.4 0.0 all-to-all-done
  87.4 9.1 %all-to-all-start.2 = ((bf16[32,16,2048]{2,1,0:T(8,128)(2,1)}), bf16[32,16,2048]{2,1,0:T(8,128)(2,1)S(1)}, u32[]{:S(2)}, u32[]{:S(2)}) async-start(bf16[32,16,2048]{2,1,0:T(8,128)(2,1)} %bitcast.85), calls=%async_computation.2 | async-start | bytes 4194304 | tf_op jit(solution)/shard_map/all_to_all | solution.py:83
  96.5 0.0 copy-done.5
  96.5 4.4 %convolution_convert_fusion = bf16[256,2048]{1,0:T(8,128)(2,1)} fusion(bf16[256,1024]{0,1:T(8,128)(2,1)S(1)} %bitcast.87, bf16[1024,2048]{1,0:T(8,128)(2,1)} %param.18), kind=kOutput, calls=%fused_computation.12 | convolution fusion | flops 1074266112 | bytes 5767168 | tf_op jit(solution)/shard_map/dot_general | solution.py:62
  101.0 44.1 %all-to-all-done.2 = bf16[32,16,2048]{2,1,0:T(8,128)(2,1)S(1)} async-done(((bf16[32,16,2048]{2,1,0:T(8,128)(2,1)}), bf16[32,16,2048]{2,1,0:T(8,128)(2,1)S(1)}, u32[]{:S(2)}, u32[]{:S(2)}) %all-to-all-start.2) | async-done | bytes 2097184 | tf_op jit(solution)/shard_map/all_to_all | solution.py:83
  145.0 3.3 %gather_fusion.1 = bf16[512,2048]{1,0:T(8,128)(2,1)} fusion(bf16[512,2048]{1,0:T(8,128)(2,1)S(1)} %bitcast.82, s32[1024]{0:T(1024)S(1)} %pad_clamp_fusion), kind=kCustom, calls=%fused_computation.1 | custom fusion | bytes 4196352 | tf_op jit(solution)/shard_map/gather | solution.py:92
  148.4 3.2 %reshape.108 = bf16[256,2,2048]{2,1,0:T(2,128)(2,1)S(1)} reshape(bf16[512,2048]{1,0:T(8,128)(2,1)} %gather_fusion.1) | data formatting | bytes 4194304 | tf_op jit(solution)/shard_map/reshape | solution.py:92
  151.5 3.0 %fusion.37 = (bf16[256,1,2048]{2,1,0:T(2,128)(2,1)S(1)}, bf16[256,1,2048]{2,1,0:T(2,128)(2,1)S(1)}) fusion(bf16[256,2,2048]{2,1,0:T(2,128)(2,1)S(1)} %reshape.108), kind=kLoop, calls=%fused_computation.68 | loop fusion | bytes 4194304 | tf_op jit(solution)/shard_map/slice | solution.py:93
  154.5 3.3 %fusion.13 = bf16[256,2048]{1,0:T(8,128)(2,1)} fusion(bf16[256,1,2048]{2,1,0:T(2,128)(2,1)S(1)} %get-tuple-element.5, bf16[256,1,2048]{2,1,0:T(2,128)(2,1)S(1)} %get-tuple-element.4, f32[256]{0:T(256)S(1)} %bitcast.92, f32[256]{0:T(256)S(1)} %bitcast.91), kind=kLoop, calls=%fused_computation.18 | loop fusion | flops 3145728 | bytes 3147776 | tf_op jit(solution)/shard_map/convert_element_type | solution.py:95
  (17 shorter events, 0.1 us)
Async XLA Ops:
  0.6 7.8 %copy-start = (bf16[256,2048]{1,0:T(8,128)(2,1)S(1)}, bf16[256,2048]{1,0:T(8,128)(2,1)}, u32[]{:S(2)}) copy-start(bf16[256,2048]{1,0:T(8,128)(2,1)} %param.19) | copy-start | bytes 3145732
  0.6 7.8 %copy-start.3 = (f32[2048]{0:T(1024)S(1)}, f32[2048]{0:T(1024)}, u32[]{:S(2)}) copy-start(f32[2048]{0:T(1024)} %param.20) | copy-start | bytes 24580
  12.1 7.3 %copy-start.1 = (bf16[1024,256]{1,0:T(8,128)(2,1)S(1)}, bf16[1024,256]{1,0:T(8,128)(2,1)}, u32[]{:S(2)}) copy-start(bf16[1024,256]{1,0:T(8,128)(2,1)} %param.14) | copy-start | bytes 1572868
  12.1 7.3 %copy-start.2 = (bf16[1024,256]{1,0:T(8,128)(2,1)S(1)}, bf16[1024,256]{1,0:T(8,128)(2,1)}, u32[]{:S(2)}) copy-start(bf16[1024,256]{1,0:T(8,128)(2,1)} %param.15) | copy-start | bytes 1572868
  12.1 56.0 %all-to-all-start.1 = ((bf16[32,16,2048]{2,1,0:T(8,128)(2,1)}), bf16[32,16,2048]{2,1,0:T(8,128)(2,1)S(1)}, u32[]{:S(2)}, u32[]{:S(2)}) async-start(bf16[32,16,2048]{2,1,0:T(8,128)(2,1)} %bitcast.14), calls=%async_computation.1 | async-start | bytes 4194304 | tf_op jit(solution)/shard_map/all_to_all | solution.py:81
  19.6 7.1 %copy-start.4 = (f32[3,256]{1,0:T(4,128)S(1)}, f32[3,256]{1,0:T(4,128)}, u32[]{:S(2)}) copy-start(f32[3,256]{1,0:T(4,128)} %param.16) | copy-start | bytes 9220
  19.7 20.4 %collective-permute-start = (bf16[2,2,256]{1,2,0:T(8,128)(2,1)S(1)}, bf16[2,2,256]{1,2,0:T(8,128)(2,1)S(1)}, u32[]{:S(2)}, u32[]{:S(2)}) collective-permute-start(bf16[2,2,256]{1,2,0:T(8,128)(2,1)S(1)} %copy.30), channel_id=1, source_target_pairs={{0,4},{4,8},{8,12},{12,16},{16,20},{20,24},{24,28},{1,5},{5,9},{9,... | collective-permute-start | bytes 6152 | tf_op jit(solution)/shard_map/ppermute | solution.py:12
  26.7 15.2 %copy-start.6 = (f32[256]{0:T(256)S(1)}, f32[256]{0:T(256)}, u32[]{:S(2)}) copy-start(f32[256]{0:T(256)} %param.17) | copy-start | bytes 3076
  68.1 19.2 %all-to-all-start = ((bf16[4,256,256]{1,2,0:T(8,128)(2,1)}), bf16[4,256,256]{1,2,0:T(8,128)(2,1)S(1)}, u32[]{:S(2)}, u32[]{:S(2)}) async-start(bf16[4,256,256]{1,2,0:T(8,128)(2,1)} %bitcast.81), calls=%async_computation | async-start | bytes 1048576 | tf_op jit(solution)/shard_map/all_to_all | solution.py:60
  87.4 9.1 %copy-start.5 = (f32[256,2]{0,1:T(2,128)S(1)}, f32[256,2]{0,1:T(2,128)}, u32[]{:S(2)}) copy-start(f32[256,2]{0,1:T(2,128)} %param.22) | copy-start | bytes 6148
  87.4 57.6 %all-to-all-start.2 = ((bf16[32,16,2048]{2,1,0:T(8,128)(2,1)}), bf16[32,16,2048]{2,1,0:T(8,128)(2,1)S(1)}, u32[]{:S(2)}, u32[]{:S(2)}) async-start(bf16[32,16,2048]{2,1,0:T(8,128)(2,1)} %bitcast.85), calls=%async_computation.2 | async-start | bytes 4194304 | tf_op jit(solution)/shard_map/all_to_all | solution.py:83
where the time goes:
time: 158 us
  waiting for transfers between devices  80.5 us (51%)
  starting transfers between devices  23.6 us (15%)
  local copies, waits for them, and re-layouts  22.1 us (14%)
  matrix products  20.2 us (13%)
  other arithmetic  10.6 us (7%)
    all_to_all x1, waiting for transfers between devices, shards(): lax.all_to_all(expert_rows(portion.reshape(-1, width), w_gate, w_up, w_do...  44.1 us
    all_to_all x1, waiting for transfers between devices, shards(): lax.all_to_all(outgoing, ('ep', 'tp'), split_axis=0, concat_axis=0, tiled...  25.1 us
    ppermute x1, waiting for transfers between devices, shifted(): return lax.ppermute(value, axis, pairs)  11.3 us
    dot_general x1, matrix products, expert_rows(): jnp.dot(hidden, w_down, preferred_element_type=jnp.float32)  9.89 us
    all_to_all x1, starting transfers between devices, shards(): lax.all_to_all(expert_rows(portion.reshape(-1, width), w_gate, w_up, w_do...  9.11 us
    all_to_all x1, starting transfers between devices, shards(): lax.all_to_all(outgoing, ('ep', 'tp'), split_axis=0, concat_axis=0, tiled...  7.33 us
    dot_general x1, matrix products, expert_rows(): gate_part = jnp.dot(inputs, w_gate, preferred_element_type=jnp.float32)  5.87 us
    unnamed x18, local copies, waits for them, and re-layouts  4.98 us
  transfers between devices with their start and end apart: 4, of which 3 were waited for; matrix products, arithmetic and copies ran while one was open for 18% of the time, Pallas kernels for 0%

commit v1 on v0

v1 whole, which is shorter than its diff:
```python
import functools

import jax
import jax.numpy as jnp
from jax import lax
from jax.experimental import pallas as pl
from jax.experimental.pallas import tpu as pltpu
from jax.sharding import PartitionSpec as P

GROUP_CH = 64
MESH = pl.DeviceIdType.MESH
BF16 = jnp.bfloat16
F32 = jnp.float32


def shifted(value, axis, by):
    count = lax.axis_size(axis)
    pairs = [(i, i + by) for i in range(count) if 0 <= i + by < count]
    return lax.ppermute(value, axis, pairs)


def round_up(value, to):
    return (value + to - 1) // to * to


def tdot(a, b):
    return lax.dot_general(a, b, (((0,), (0,)), ((), ())), preferred_element_type=F32)


def experts_kernel(
    n_ep, n_tp, slot, pad_slot, chunks,
    x_ref, gain_ref, ids_ref, rw_ref, wg_hbm, wu_hbm, wd_hbm,
    out_ref,
    wg, wu, wd, norm, place, sorted_rows, landed, picked, xin, hidden, obuf, comb, sums, fin,
    w_sem, d_send, d_recv, p_send, p_recv, r_send, r_recv, f_send, f_recv,
):
    me_e = lax.axis_index("ep")
    me_t = lax.axis_index("tp")
    tok, width = x_ref.shape
    rows = tok // n_ep
    slots = n_tp * pad_slot
    meta = norm.shape[1] - width
    weights = [
        pltpu.make_async_copy(src.at[0], dst, w_sem.at[i])
        for i, (src, dst) in enumerate(((wg_hbm, wg), (wu_hbm, wu), (wd_hbm, wd)))
    ]
    for copy in weights:
        copy.start()

    def ep_peer(k):
        return lax.rem(me_e + k, n_ep)

    def tp_peer(j):
        return lax.rem(me_t + j, n_tp)

    barrier = pltpu.get_barrier_semaphore()
    for k in range(1, n_ep):
        pl.semaphore_signal(
            barrier, inc=1, device_id={"ep": ep_peer(k), "tp": me_t}, device_id_type=MESH
        )
    for j in range(1, n_tp):
        pl.semaphore_signal(
            barrier, inc=1, device_id={"ep": me_e, "tp": tp_peer(j)}, device_id_type=MESH
        )

    experts = n_ep * n_tp
    ids0, ids1 = ids_ref[:, 0:1], ids_ref[:, 1:2]
    lane_e = lax.broadcasted_iota(jnp.int32, (tok, experts), 1)
    hit0 = (ids0 == lane_e).astype(F32)
    hit1 = (ids1 == lane_e).astype(F32)
    both = (hit0 + hit1).astype(BF16)
    lower = (
        lax.broadcasted_iota(jnp.int32, (tok, tok), 1) < lax.broadcasted_iota(jnp.int32, (tok, tok), 0)
    ).astype(BF16)
    before = jnp.dot(lower, both, preferred_element_type=F32)
    rank0 = jnp.sum(before * hit0, axis=1, keepdims=True).astype(jnp.int32)
    rank1 = jnp.sum(before * hit1, axis=1, keepdims=True).astype(jnp.int32)
    group = ids0 // n_tp
    in_group = ((ids0 // n_tp) == (lane_e // n_tp)).astype(F32)
    rank_g = jnp.sum(before * in_group, axis=1, keepdims=True).astype(jnp.int32) // 2
    place[...] = (
        (group * rows + rank_g) == lax.broadcasted_iota(jnp.int32, (tok, tok), 1)
    ).astype(BF16)
    cell0 = (ids0 - group * n_tp) * pad_slot + rank0
    cell1 = (ids1 - group * n_tp) * pad_slot + rank1
    lane_s = lax.broadcasted_iota(jnp.int32, (tok, slots), 1)
    at0 = (cell0 == lane_s).astype(F32)
    at1 = (cell1 == lane_s).astype(F32)
    weight = at0 * rw_ref[:, 0:1] + at1 * rw_ref[:, 1:2]
    high = weight.astype(BF16)
    low = (weight - high.astype(F32)).astype(BF16)
    packed = [high, low, (at0 + at1).astype(BF16)]
    if meta > 3 * slots:
        packed.append(jnp.zeros((tok, meta - 3 * slots), BF16))
    norm[:, width:] = jnp.concatenate(packed, axis=1)

    step = 32

    @pl.loop(0, tok // step)
    def _(i):
        at = pl.ds(pl.multiple_of(i * step, step), step)
        wide = x_ref[at, :].astype(F32)
        scale = lax.rsqrt(jnp.mean(wide * wide, axis=-1, keepdims=True) + 1e-06)
        norm[at, 0:width] = (wide * scale * gain_ref[...]).astype(BF16)

    sorted_rows[...] = tdot(place[...], norm[...]).astype(BF16)

    pl.semaphore_wait(barrier, n_ep - 1 + n_tp - 1)

    dispatch = []
    for k in range(1, n_ep):
        to = ep_peer(k)
        copy = pltpu.make_async_remote_copy(
            src_ref=sorted_rows.at[pl.ds(pl.multiple_of(to * rows, rows), rows)],
            dst_ref=landed.at[k],
            send_sem=d_send.at[k],
            recv_sem=d_recv.at[k],
            device_id={"ep": to, "tp": me_t},
            device_id_type=MESH,
        )
        copy.start()
        dispatch.append(copy)
    landed[0] = sorted_rows[pl.ds(pl.multiple_of(me_e * rows, rows), rows), :]

    spread = {}
    for k in range(n_ep):
        if k:
            dispatch[k - 1].wait_recv()
        chosen = landed[k, :, pl.ds(width + 2 * slots, slots)]
        picked[k] = tdot(chosen, landed[k, :, 0:width]).astype(BF16)
        for j in range(1, n_tp):
            to = tp_peer(j)
            copy = pltpu.make_async_remote_copy(
                src_ref=picked.at[k, pl.ds(pl.multiple_of(to * pad_slot, pad_slot), pad_slot)],
                dst_ref=xin.at[pl.ds((k * n_tp + j) * pad_slot, pad_slot)],
                send_sem=p_send.at[k, j],
                recv_sem=p_recv.at[k, j],
                device_id={"ep": me_e, "tp": to},
                device_id_type=MESH,
            )
            copy.start()
            spread[k, j] = copy
        xin[pl.ds(k * n_tp * pad_slot, pad_slot), :] = picked[
            k, pl.ds(pl.multiple_of(me_t * pad_slot, pad_slot), pad_slot), :
        ]

    for copy in weights:
        copy.wait()
    hid = wg.shape[1]
    per = n_ep // chunks
    many = per * n_tp * pad_slot
    back = {}
    mine = pl.ds(pl.multiple_of(me_t * pad_slot, pad_slot), pad_slot)
    for c in range(chunks):
        for k in range(c * per, (c + 1) * per):
            for j in range(1, n_tp):
                spread[k, j].wait_recv()
        span = pl.ds(c * many, many)

        @pl.loop(0, hid // 256)
        def _(f):
            cols = pl.ds(pl.multiple_of(f * 256, 256), 256)
            gate = jnp.dot(xin[span, :], wg[:, cols], preferred_element_type=F32)
            up = jnp.dot(xin[span, :], wu[:, cols], preferred_element_type=F32)
            hidden[:, cols] = (gate / (1.0 + jnp.exp(-gate)) * up).astype(BF16)

        @pl.loop(0, width // 512)
        def _(f):
            cols = pl.ds(pl.multiple_of(f * 512, 512), 512)
            obuf[span, cols] = jnp.dot(
                hidden[...], wd[:, cols], preferred_element_type=F32
            ).astype(BF16)

        for k in range(c * per, (c + 1) * per):
            for j in range(1, n_tp):
                to = tp_peer(n_tp - j)
                copy = pltpu.make_async_remote_copy(
                    src_ref=obuf.at[pl.ds((k * n_tp + j) * pad_slot, pad_slot)],
                    dst_ref=comb.at[k, mine],
                    send_sem=r_send.at[k, j],
                    recv_sem=r_recv.at[k, j],
                    device_id={"ep": me_e, "tp": to},
                    device_id_type=MESH,
                )
                copy.start()
                back[k, j] = copy
            comb[k, mine, :] = obuf[pl.ds(k * n_tp * pad_slot, pad_slot), :]

    home = []
    here = pl.ds(pl.multiple_of(me_e * rows, rows), rows)
    order = list(range(1, n_ep)) + [0]
    for k in order:
        for j in range(1, n_tp):
            back[k, j].wait_recv()
        total = jnp.dot(
            landed[k, :, pl.ds(width, slots)], comb[k], preferred_element_type=F32
        ) + jnp.dot(
            landed[k, :, pl.ds(width + slots, slots)], comb[k], preferred_element_type=F32
        )
        if k == 0:
            fin[here, :] = total.astype(BF16)
            continue
        sums[k] = total.astype(BF16)
        copy = pltpu.make_async_remote_copy(
            src_ref=sums.at[k],
            dst_ref=fin.at[here],
            send_sem=f_send.at[k],
            recv_sem=f_recv.at[k],
            device_id={"ep": ep_peer(n_ep - k), "tp": me_t},
            device_id_type=MESH,
        )
        copy.start()
        home.append(copy)
    for copy in home:
        copy.wait_recv()

    @pl.loop(0, width // 512)
    def _(f):
        cols = pl.ds(pl.multiple_of(f * 512, 512), 512)
        out_ref[:, cols] = jnp.dot(
            place[...], fin[:, cols], preferred_element_type=F32
        ).astype(BF16)

    for copy in dispatch + list(spread.values()) + list(back.values()) + home:
        copy.wait_send()


def experts(moe_in, moe_gain, route_ids, route_weight, gate_w, up_w, down_w):
    n_ep, n_tp = lax.axis_size("ep"), lax.axis_size("tp")
    tok, width = moe_in.shape
    hid = gate_w.shape[2]
    slot = 2 * tok // (n_ep * n_tp)
    pad_slot = round_up(slot, 16)
    rows = tok // n_ep
    slots = n_tp * pad_slot
    meta = round_up(3 * slots, 128)
    total = n_ep * slots
    chunks = 2
    vm = pl.BlockSpec(memory_space=pltpu.VMEM)
    hbm = pl.BlockSpec(memory_space=pl.ANY)
    dma = pltpu.SemaphoreType.DMA
    return pl.pallas_call(
        functools.partial(experts_kernel, n_ep, n_tp, slot, pad_slot, chunks),
        out_shape=jax.ShapeDtypeStruct((tok, width), BF16),
        in_specs=[vm, vm, vm, vm, hbm, hbm, hbm],
        out_specs=vm,
        scratch_shapes=[
            pltpu.VMEM((width, hid), BF16),
            pltpu.VMEM((width, hid), BF16),
            pltpu.VMEM((hid, width), BF16),
            pltpu.VMEM((tok, width + meta), BF16),
            pltpu.VMEM((tok, tok), BF16),
            pltpu.VMEM((tok, width + meta), BF16),
            pltpu.VMEM((n_ep, rows, width + meta), BF16),
            pltpu.VMEM((n_ep, slots, width), BF16),
            pltpu.VMEM((total, width), BF16),
            pltpu.VMEM((total // chunks, hid), BF16),
            pltpu.VMEM((total, width), BF16),
            pltpu.VMEM((n_ep, slots, width), BF16),
            pltpu.VMEM((n_ep, rows, width), BF16),
            pltpu.VMEM((tok, width), BF16),
            dma((3,)),
            dma((n_ep,)),
            dma((n_ep,)),
            dma((n_ep, n_tp)),
            dma((n_ep, n_tp)),
            dma((n_ep, n_tp)),
            dma((n_ep, n_tp)),
            dma((n_ep,)),
            dma((n_ep,)),
        ],
        compiler_params=pltpu.CompilerParams(
            collective_id=0, has_side_effects=True, vmem_limit_bytes=60 * 1024 * 1024
        ),
        cost_estimate=pl.CostEstimate(
            flops=6 * total * width * hid, bytes_accessed=8 * width * hid, transcendentals=0
        ),
    )(moe_in, moe_gain.reshape(1, width), route_ids, route_weight, gate_w, up_w, down_w)


def shards(
    out_gate,
    in_gate,
    conv_input,
    conv_taps,
    group_gain,
    mix_out_w,
    moe_in,
    moe_gain,
    route_ids,
    route_weight,
    gate_w,
    up_w,
    down_w,
):
    rows_ep, channels = in_gate.shape
    member_count = lax.axis_size("tp")
    group_count = lax.axis_size("ep")
    reach = conv_taps.shape[0] - 1
    edge_rows = jnp.stack([in_gate[rows_ep - reach :], conv_input[rows_ep - reach :]])
    earlier = shifted(edge_rows, "ep", 1)
    product = in_gate.astype(jnp.float32) * conv_input.astype(jnp.float32)
    before_rows = earlier[0].astype(jnp.float32) * earlier[1].astype(jnp.float32)
    padded = jnp.concatenate([before_rows, product], axis=0)
    convolved = jnp.zeros_like(product)
    for tap in range(reach + 1):
        convolved = convolved + conv_taps[tap] * padded[tap : tap + rows_ep]
    gated = out_gate.astype(jnp.float32) * convolved
    grouped = gated.reshape(rows_ep, channels // GROUP_CH, GROUP_CH)
    inv_rms = lax.rsqrt(jnp.mean(grouped * grouped, axis=-1, keepdims=True) + 1e-06)
    normed = ((grouped * inv_rms).reshape(rows_ep, channels) * group_gain).astype(jnp.bfloat16)
    blocks = normed.reshape(member_count, rows_ep // member_count, channels)
    portion = lax.all_to_all(blocks, "tp", split_axis=0, concat_axis=2, tiled=True)
    flat_rows = portion.reshape(-1, portion.shape[2])
    projected = jnp.dot(flat_rows, mix_out_w, preferred_element_type=jnp.float32).astype(
        jnp.bfloat16
    )
    mixed = projected.reshape(portion.shape[0], portion.shape[1], -1)
    mixed = mixed.reshape(-1, mixed.shape[2])
    moe_out = experts(moe_in, moe_gain, route_ids, route_weight, gate_w, up_w, down_w)
    return (mixed, moe_out)


def solution(mesh):
    in_specs = (
        P("ep", "tp"),
        P("ep", "tp"),
        P("ep", "tp"),
        P(None, "tp"),
        P("tp"),
        P(),
        P(("ep", "tp"), None),
        P(),
        P(("ep", "tp"), None),
        P(("ep", "tp"), None),
        P(("ep", "tp"), None, None),
        P(("ep", "tp"), None, None),
        P(("ep", "tp"), None, None),
    )
    out_specs = (P(("ep", "tp"), None), P(("ep", "tp"), None))
    return jax.shard_map(shards, mesh=mesh, in_specs=in_specs, out_specs=out_specs, check_vma=False)
```

time: 158 us -> 102 us (0.65)
  waiting for transfers between devices: 80.5 us -> 0.01 us
  Pallas kernels: 0 us -> 79.4 us
  matrix products: 20.2 us -> 4.51 us
  starting transfers between devices: 23.6 us -> 8.35 us
  local copies, waits for them, and re-layouts: 22.1 us -> 7.09 us
  other arithmetic: 10.6 us -> 1.23 us
    pallas_call x0 -> x1, Pallas kernels: none -> 79.4 us  [experts(): pl.pallas_call(functools.partial(experts_kernel, n_ep, n_tp, slot, pad_sl...]
    all_to_all x2 -> x0, waiting for transfers between devices: 69.2 us -> none  [the longest x1 44.1 us: shards(): lax.all_to_all(expert_rows(portion.reshape(-1, width), w_gate, w_up, w_do...]
    all_to_all x2 -> x0, starting transfers between devices: 16.4 us -> none  [the longest x1 9.11 us: shards(): lax.all_to_all(expert_rows(portion.reshape(-1, width), w_gate, w_up, w_do...]
    dot_general x2 -> x0, matrix products: 15.8 us -> none  [the longest x1 9.89 us: expert_rows(): jnp.dot(hidden, w_down, preferred_element_type=jnp.float32)]
    ppermute x1, waiting for transfers between devices: 11.3 us -> 0.01 us  [shifted(): return lax.ppermute(value, axis, pairs)]
    gather x2 -> x0, local copies, waits for them, and re-layouts: 6.69 us -> none  [the longest x1 3.35 us: shards(): outgoing = expert_in[sources].reshape(expert_count, slot_count, width)]
    convert_element_type x3 -> x0, other arithmetic: 3.62 us -> none  [the longest x1 3.3 us: shards(): (first_out * route_weight[:, 0:1] + second * route_weight[:, 1:2]).astype...]
    slice x3 -> x0, local copies, waits for them, and re-layouts: 3.2 us -> none  [the longest x1 2.97 us: shards(): first_out = results[:, 0].astype(jnp.float32)]
  transfers between devices with their start and end apart: 4 -> 2, of which waited for: 3 -> 0; matrix products, arithmetic and copies ran while one was open for 18% -> 4% of each run, Pallas kernels for 0% -> 78%
where the time goes in v1:
time: 102 us; the launch traced here: 101 us
  Pallas kernels  79.4 us (78%)
  starting transfers between devices  8.35 us (8%)
  local copies, waits for them, and re-layouts  7.09 us (7%)
  matrix products  4.51 us (4%)
  other arithmetic  1.23 us (1%)
    pallas_call x1, Pallas kernels, experts(): pl.pallas_call(functools.partial(experts_kernel, n_ep, n_tp, slot, pad_sl...  79.4 us
    unnamed x18, local copies, waits for them, and re-layouts  5.3 us
    ppermute x1, starting transfers between devices, shifted(): return lax.ppermute(value, axis, pairs)  4.88 us
    dot_general x1, matrix products, shards(): jnp.dot(flat_rows, mix_out_w, preferred_element_type=jnp.float32)  4.51 us
    all_to_all x1, starting transfers between devices, shards(): lax.all_to_all(blocks, 'tp', split_axis=0, concat_axis=2, tiled=True)  3.47 us
  transfers between devices with their start and end apart: 2, of which 0 were waited for; matrix products, arithmetic and copies ran while one was open for 4% of the time, Pallas kernels for 78%

profile of v1, /device:TPU:0, one launch (start us, length us, event | category | flops | bytes accessed | tf_op | source)
XLA Modules:
  0.0 101.4 jit_solution(5069948834283896950)
XLA Ops:
  0.6 0.0 copy-start.2
  0.6 0.0 copy-start.3
  0.7 0.0 copy-start.4
  0.7 0.0 copy-start.1
  0.7 0.8 slice_bitcast_fusion
  1.5 0.2 copy.26
  1.6 0.0 copy-start.5
  1.7 4.9 %collective-permute-start = (bf16[2,2,256]{1,2,0:T(8,128)(2,1)S(1)}, bf16[2,2,256]{1,2,0:T(8,128)(2,1)S(1)}, u32[]{:S(2)}, u32[]{:S(2)}) collective-permute-start(bf16[2,2,256]{1,2,0:T(8,128)(2,1)S(1)} %copy.26), channel_id=1, source_target_pairs={{0,4},{4,8},{8,12},{12,16},{16,20},{20,24},{24,28},{1,5},{5,9},{9,... | collective-permute-start | bytes 6152 | tf_op jit(solution)/shard_map/ppermute | solution.py:19
  6.5 1.2 %copy.27 = bf16[1024,256]{0,1:T(8,128)(2,1)S(1)} copy(bf16[1024,256]{1,0:T(8,128)(2,1)} %param.14) | data formatting | bytes 1048576 | tf_op args[1]
  7.8 1.2 %copy.28 = bf16[1024,256]{0,1:T(8,128)(2,1)S(1)} copy(bf16[1024,256]{1,0:T(8,128)(2,1)} %param.15) | data formatting | bytes 1048576 | tf_op args[2]
  9.0 0.2 convert_multiply_fusion
  9.2 0.0 copy-done.2
  9.2 0.0 copy-done.3
  9.3 0.8 copy.30.ids_ref
  10.1 0.0 copy-done.4
  10.1 0.8 copy.31.rw_ref
  10.9 0.0 copy-done.1
  10.9 0.2 copy.25
  11.1 0.0 collective-permute-done
  11.1 0.8 bitcast_reduce_fusion
  12.0 0.0 copy-done.5
  12.0 0.2 fusion.7
  12.2 0.8 copy.34
  13.0 3.5 %all-to-all-start = ((bf16[4,256,256]{1,2,0:T(8,128)(2,1)}), bf16[4,256,256]{1,2,0:T(8,128)(2,1)S(1)}, u32[]{:S(2)}, u32[]{:S(2)}) async-start(bf16[4,256,256]{1,2,0:T(8,128)(2,1)} %bitcast.28), calls=%async_computation | async-start | bytes 1048576 | tf_op jit(solution)/shard_map/all_to_all | solution.py:313
  16.5 79.4 %shard_map.140 = bf16[256,2048]{1,0:T(8,128)(2,1)} custom-call(bf16[256,2048]{1,0:T(8,128)(2,1)} %x_ref.1, f32[1,2048]{1,0:T(1,128)} %bitcast.34, s32[256,2]{1,0:T(8,128)} %copy.30.ids_ref, f32[256,2]{1,0:T(8,128)} %copy.31.rw_ref, bf16[1,2048,1024]{2,1,0:T(8,128)(2,1)} %wg_hbm.1, bf16[1,2048,1024]{2,1,0:T(8,128)(2,1)} %wu_hbm.1, bf16[1,1024,2048]{2,1,0:T(8,128)(2,1)} %wd_hbm.1), custom_call_target="tpu_custom_call" | custom-call | flops 6442450944 | bytes 16777216 | tf_op jit(solution)/shard_map/pallas_call | solution.py:242
  95.9 0.0 copy-start
  95.9 0.0 all-to-all-done
  95.9 4.5 %convolution_convert_fusion = bf16[256,2048]{1,0:T(8,128)(2,1)} fusion(bf16[256,1024]{0,1:T(8,128)(2,1)S(1)} %bitcast.30, bf16[1024,2048]{1,0:T(8,128)(2,1)} %param.18), kind=kOutput, calls=%fused_computation | convolution fusion | flops 1074266112 | bytes 5767168 | tf_op jit(solution)/shard_map/dot_general | solution.py:315
  100.4 0.0 copy-done
  100.4 1.0 copy.36
  (4 shorter events, 0.0 us)
Async XLA Ops:
  0.6 8.6 %copy-start.2 = (f32[3,256]{1,0:T(4,128)S(1)}, f32[3,256]{1,0:T(4,128)}, u32[]{:S(2)}) copy-start(f32[3,256]{1,0:T(4,128)} %param.16) | copy-start | bytes 9220
  0.6 8.6 %copy-start.3 = (s32[256,2]{0,1:T(2,128)S(1)}, s32[256,2]{0,1:T(2,128)}, u32[]{:S(2)}) copy-start(s32[256,2]{0,1:T(2,128)} %param.21) | copy-start | bytes 6148
  0.7 9.4 %copy-start.4 = (f32[256,2]{0,1:T(2,128)S(1)}, f32[256,2]{0,1:T(2,128)}, u32[]{:S(2)}) copy-start(f32[256,2]{0,1:T(2,128)} %param.22) | copy-start | bytes 6148
  0.7 10.2 %copy-start.1 = (bf16[1024,256]{1,0:T(8,128)(2,1)S(1)}, bf16[1024,256]{1,0:T(8,128)(2,1)}, u32[]{:S(2)}) copy-start(bf16[1024,256]{1,0:T(8,128)(2,1)} %param.13) | copy-start | bytes 1572868
  1.6 10.3 %copy-start.5 = (f32[256]{0:T(256)S(1)}, f32[256]{0:T(256)}, u32[]{:S(2)}) copy-start(f32[256]{0:T(256)} %param.17) | copy-start | bytes 3076
  1.7 9.4 %collective-permute-start = (bf16[2,2,256]{1,2,0:T(8,128)(2,1)S(1)}, bf16[2,2,256]{1,2,0:T(8,128)(2,1)S(1)}, u32[]{:S(2)}, u32[]{:S(2)}) collective-permute-start(bf16[2,2,256]{1,2,0:T(8,128)(2,1)S(1)} %copy.26), channel_id=1, source_target_pairs={{0,4},{4,8},{8,12},{12,16},{16,20},{20,24},{24,28},{1,5},{5,9},{9,... | collective-permute-start | bytes 6152 | tf_op jit(solution)/shard_map/ppermute | solution.py:19
  13.0 82.9 %all-to-all-start = ((bf16[4,256,256]{1,2,0:T(8,128)(2,1)}), bf16[4,256,256]{1,2,0:T(8,128)(2,1)S(1)}, u32[]{:S(2)}, u32[]{:S(2)}) async-start(bf16[4,256,256]{1,2,0:T(8,128)(2,1)} %bitcast.28), calls=%async_computation | async-start | bytes 1048576 | tf_op jit(solution)/shard_map/all_to_all | solution.py:313
  95.9 4.5 %copy-start = (bf16[256,2048]{1,0:T(8,128)(2,1)S(1)}, bf16[256,2048]{1,0:T(8,128)(2,1)}, u32[]{:S(2)}) copy-start(bf16[256,2048]{1,0:T(8,128)(2,1)} %shard_map.140) | copy-start | bytes 3145732

commit v2 on v1

--- a/solution.py
+++ b/solution.py
@@ -29,10 +29,10 @@
 
 def experts_kernel(
     n_ep, n_tp, slot, pad_slot, chunks,
-    x_ref, gain_ref, ids_ref, rw_ref, wg_hbm, wu_hbm, wd_hbm,
-    out_ref,
-    wg, wu, wd, norm, place, sorted_rows, landed, picked, xin, hidden, obuf, comb, sums, fin,
-    w_sem, d_send, d_recv, p_send, p_recv, r_send, r_recv, f_send, f_recv,
+    x_ref, gain_ref, ids_ref, rw_ref, normed_ref, wg_hbm, wu_hbm, wd_hbm, wm_hbm,
+    mixed_ref, out_ref,
+    wg, wu, wd, wm, norm, place, sorted_rows, landed, picked, xin, hidden, comb, sums, fin, mixin,
+    w_sem, m_send, m_recv, d_send, d_recv, p_send, p_recv, r_send, r_recv, f_send, f_recv,
 ):
     me_e = lax.axis_index("ep")
     me_t = lax.axis_index("tp")
@@ -44,6 +44,7 @@
         pltpu.make_async_copy(src.at[0], dst, w_sem.at[i])
         for i, (src, dst) in enumerate(((wg_hbm, wg), (wu_hbm, wu), (wd_hbm, wd)))
     ]
+    weights.append(pltpu.make_async_copy(wm_hbm, wm, w_sem.at[3]))
     for copy in weights:
         copy.start()
 
@@ -120,6 +121,22 @@
         )
         copy.start()
         dispatch.append(copy)
+    part, lanes = mixin.shape[0], normed_ref.shape[1]
+    own_lanes = pl.ds(pl.multiple_of(me_t * lanes, lanes), lanes)
+    mixes = []
+    for j in range(1, n_tp):
+        to = tp_peer(j)
+        copy = pltpu.make_async_remote_copy(
+            src_ref=normed_ref.at[pl.ds(pl.multiple_of(to * part, part), part)],
+            dst_ref=mixin.at[:, own_lanes],
+            send_sem=m_send.at[j],
+            recv_sem=m_recv.at[j],
+            device_id={"ep": me_e, "tp": to},
+            device_id_type=MESH,
+        )
+        copy.start()
+        mixes.append(copy)
+    mixin[:, own_lanes] = normed_ref[pl.ds(pl.multiple_of(me_t * part, part), part), :]
     landed[0] = sorted_rows[pl.ds(pl.multiple_of(me_e * rows, rows), rows), :]
 
     spread = {}
@@ -146,6 +163,16 @@
 
     for copy in weights:
         copy.wait()
+    for copy in mixes:
+        copy.wait_recv()
+
+    @pl.loop(0, width // 512)
+    def _(f):
+        cols = pl.ds(pl.multiple_of(f * 512, 512), 512)
+        mixed_ref[:, cols] = jnp.dot(
+            mixin[...], wm[:, cols], preferred_element_type=F32
+        ).astype(BF16)
+
     hid = wg.shape[1]
     per = n_ep // chunks
     many = per * n_tp * pad_slot
@@ -167,7 +194,7 @@
         @pl.loop(0, width // 512)
         def _(f):
             cols = pl.ds(pl.multiple_of(f * 512, 512), 512)
-            obuf[span, cols] = jnp.dot(
+            xin[span, cols] = jnp.dot(
                 hidden[...], wd[:, cols], preferred_element_type=F32
             ).astype(BF16)
 
@@ -175,7 +202,7 @@
             for j in range(1, n_tp):
                 to = tp_peer(n_tp - j)
                 copy = pltpu.make_async_remote_copy(
-                    src_ref=obuf.at[pl.ds((k * n_tp + j) * pad_slot, pad_slot)],
+                    src_ref=xin.at[pl.ds((k * n_tp + j) * pad_slot, pad_slot)],
                     dst_ref=comb.at[k, mine],
                     send_sem=r_send.at[k, j],
                     recv_sem=r_recv.at[k, j],
@@ -184,7 +211,7 @@
                 )
                 copy.start()
                 back[k, j] = copy
-            comb[k, mine, :] = obuf[pl.ds(k * n_tp * pad_slot, pad_slot), :]
+            comb[k, mine, :] = xin[pl.ds(k * n_tp * pad_slot, pad_slot), :]
 
     home = []
     here = pl.ds(pl.multiple_of(me_e * rows, rows), rows)
@@ -221,11 +248,11 @@
             place[...], fin[:, cols], preferred_element_type=F32
         ).astype(BF16)
 
-    for copy in dispatch + list(spread.values()) + list(back.values()) + home:
+    for copy in dispatch + list(spread.values()) + list(back.values()) + home + mixes:
         copy.wait_send()
 
 
-def experts(moe_in, moe_gain, route_ids, route_weight, gate_w, up_w, down_w):
+def experts(moe_in, moe_gain, route_ids, route_weight, normed, gate_w, up_w, down_w, mix_out_w):
     n_ep, n_tp = lax.axis_size("ep"), lax.axis_size("tp")
     tok, width = moe_in.shape
     hid = gate_w.shape[2]
@@ -236,18 +263,24 @@
     meta = round_up(3 * slots, 128)
     total = n_ep * slots
     chunks = 2
+    part = normed.shape[0] // n_tp
+    channels = mix_out_w.shape[0]
     vm = pl.BlockSpec(memory_space=pltpu.VMEM)
     hbm = pl.BlockSpec(memory_space=pl.ANY)
     dma = pltpu.SemaphoreType.DMA
     return pl.pallas_call(
         functools.partial(experts_kernel, n_ep, n_tp, slot, pad_slot, chunks),
-        out_shape=jax.ShapeDtypeStruct((tok, width), BF16),
-        in_specs=[vm, vm, vm, vm, hbm, hbm, hbm],
-        out_specs=vm,
+        out_shape=[
+            jax.ShapeDtypeStruct((part, width), BF16),
+            jax.ShapeDtypeStruct((tok, width), BF16),
+        ],
+        in_specs=[vm, vm, vm, vm, vm, hbm, hbm, hbm, hbm],
+        out_specs=[vm, vm],
         scratch_shapes=[
             pltpu.VMEM((width, hid), BF16),
             pltpu.VMEM((width, hid), BF16),
             pltpu.VMEM((hid, width), BF16),
+            pltpu.VMEM((channels, width), BF16),
             pltpu.VMEM((tok, width + meta), BF16),
             pltpu.VMEM((tok, tok), BF16),
             pltpu.VMEM((tok, width + meta), BF16),
@@ -255,11 +288,13 @@
             pltpu.VMEM((n_ep, slots, width), BF16),
             pltpu.VMEM((total, width), BF16),
             pltpu.VMEM((total // chunks, hid), BF16),
-            pltpu.VMEM((total, width), BF16),
             pltpu.VMEM((n_ep, slots, width), BF16),
             pltpu.VMEM((n_ep, rows, width), BF16),
             pltpu.VMEM((tok, width), BF16),
-            dma((3,)),
+            pltpu.VMEM((part, channels), BF16),
+            dma((4,)),
+            dma((n_tp,)),
+            dma((n_tp,)),
             dma((n_ep,)),
             dma((n_ep,)),
             dma((n_ep, n_tp)),
@@ -275,7 +310,7 @@
         cost_estimate=pl.CostEstimate(
             flops=6 * total * width * hid, bytes_accessed=8 * width * hid, transcendentals=0
         ),
-    )(moe_in, moe_gain.reshape(1, width), route_ids, route_weight, gate_w, up_w, down_w)
+    )(moe_in, moe_gain.reshape(1, width), route_ids, route_weight, normed, gate_w, up_w, down_w, mix_out_w)
 
 
 def shards(
@@ -309,15 +344,9 @@
     grouped = gated.reshape(rows_ep, channels // GROUP_CH, GROUP_CH)
     inv_rms = lax.rsqrt(jnp.mean(grouped * grouped, axis=-1, keepdims=True) + 1e-06)
     normed = ((grouped * inv_rms).reshape(rows_ep, channels) * group_gain).astype(jnp.bfloat16)
-    blocks = normed.reshape(member_count, rows_ep // member_count, channels)
-    portion = lax.all_to_all(blocks, "tp", split_axis=0, concat_axis=2, tiled=True)
-    flat_rows = portion.reshape(-1, portion.shape[2])
-    projected = jnp.dot(flat_rows, mix_out_w, preferred_element_type=jnp.float32).astype(
-        jnp.bfloat16
+    mixed, moe_out = experts(
+        moe_in, moe_gain, route_ids, route_weight, normed, gate_w, up_w, down_w, mix_out_w
     )
-    mixed = projected.reshape(portion.shape[0], portion.shape[1], -1)
-    mixed = mixed.reshape(-1, mixed.shape[2])
-    moe_out = experts(moe_in, moe_gain, route_ids, route_weight, gate_w, up_w, down_w)
     return (mixed, moe_out)
 
 

time: 102 us -> 99.3 us (0.974)
  matrix products: 4.51 us -> 0 us
  starting transfers between devices: 8.35 us -> 4.87 us
  local copies, waits for them, and re-layouts: 7.09 us -> 9.85 us
  other arithmetic: 1.23 us -> 3.83 us
    dot_general x1 -> x0, matrix products: 4.51 us -> none  [shards(): jnp.dot(flat_rows, mix_out_w, preferred_element_type=jnp.float32)]
    all_to_all x1 -> x0, starting transfers between devices: 3.47 us -> none  [shards(): lax.all_to_all(blocks, 'tp', split_axis=0, concat_axis=2, tiled=True)]
    unnamed x18 -> x6, local copies, waits for them, and re-layouts: 5.3 us -> 7.56 us
    mul x0 -> x1, other arithmetic: none -> 1.46 us  [shards(): grouped * grouped]
    mul x1, other arithmetic: 0.17 us -> 1.31 us  [shards(): product = in_gate.astype(jnp.float32) * conv_input.astype(jnp.float32)]
  transfers between devices with their start and end apart: 2 -> 1, of which waited for: 0 -> 0; matrix products, arithmetic and copies ran while one was open for 4% -> 5% of each run, Pallas kernels for 78% -> 0%
where the time goes in v2:
time: 99.3 us; the launch traced here: 98.9 us
  Pallas kernels  79.6 us (80%)
  local copies, waits for them, and re-layouts  9.85 us (10%)
  starting transfers between devices  4.87 us (5%)
  other arithmetic  3.83 us (4%)
    pallas_call x1, Pallas kernels, experts(): pl.pallas_call(functools.partial(experts_kernel, n_ep, n_tp, slot, pad_sl...  79.6 us
    unnamed x6, local copies, waits for them, and re-layouts  7.56 us
    ppermute x1, starting transfers between devices, shifted(): return lax.ppermute(value, axis, pairs)  4.87 us
  transfers between devices with their start and end apart: 1, of which 0 were waited for; matrix products, arithmetic and copies ran while one was open for 5% of the time, Pallas kernels for 0%

profile of v2, /device:TPU:0, one launch (start us, length us, event | category | flops | bytes accessed | tf_op | source)
XLA Modules:
  0.0 98.9 jit_solution(8738734754548582155)
XLA Ops:
  0.6 0.7 slice_bitcast_fusion
  1.4 4.9 %collective-permute-start = (bf16[2,2,256]{2,1,0:T(2,128)(2,1)S(1)}, bf16[2,2,256]{2,1,0:T(2,128)(2,1)S(1)}, u32[]{:S(2)}, u32[]{:S(2)}) collective-permute-start(bf16[2,2,256]{2,1,0:T(2,128)(2,1)S(1)} %pad_maximum_fusion.1), channel_id=1, source_target_pairs={{0,4},{4,8},{8,12},{12,16},{16,20},{20,24},{24,28},{1,5},{5,9},{9,... | collective-permute-start | bytes 6152 | tf_op jit(solution)/shard_map/ppermute | solution.py:19
  6.2 1.3 %convert_multiply_fusion = f32[1024,256]{1,0:T(8,128)S(1)} fusion(bf16[1024,256]{1,0:T(8,128)(2,1)} %param.15, bf16[1024,256]{1,0:T(8,128)(2,1)} %param.14), kind=kLoop, calls=%fused_computation.11 | loop fusion | flops 786432 | bytes 2097152 | tf_op jit(solution)/shard_map/mul | solution.py:337
  7.6 0.8 fusion.8
  8.4 1.5 %copy.19.ids_ref = s32[256,2]{1,0:T(8,128)} copy(s32[256,2]{0,1:T(2,128)} %param.21) | data formatting | bytes 4096 | tf_op args[8]
  9.8 1.5 %copy.20.rw_ref = f32[256,2]{1,0:T(8,128)} copy(f32[256,2]{0,1:T(2,128)} %param.22) | data formatting | bytes 4096 | tf_op args[9]
  11.3 0.0 collective-permute-done
  11.3 0.0 copy-start
  11.3 1.5 %fusion.6 = (f32[1024,256]{1,0:T(8,128)S(1)}, f32[1024,256]{1,0:T(8,128)S(1)}) fusion(f32[1024,256]{1,0:T(8,128)S(1)} %convert_multiply_fusion, f32[256]{0:T(256)S(1)} %bitcast.15, f32[2,256]{1,0:T(2,128)S(1)} %multiply_bitcast_fusion, f32[256]{0:T(256)S(1)} %bitcast.16, f32[256]{0:T(256)S(1)} %bitcast.14, bf16[1024,256]{1,0:T(8,128)(2,1)} %param.13), kind=kLoop, calls=%fused_computation.17 | loop fusion | flops 2621440 | bytes 3675136 | tf_op jit(solution)/shard_map/mul | solution.py:345
  12.8 0.3 copy.17
  13.1 0.1 bitcast_reduce_fusion
  13.2 0.1 mul.82
  13.4 0.3 copy.18
  13.7 0.0 copy-done
  13.7 0.9 multiply_convert_fusion.normed_ref
  14.6 79.6 %shard_map.140 = (bf16[256,2048]{1,0:T(8,128)(2,1)}, bf16[256,2048]{1,0:T(8,128)(2,1)}) custom-call(bf16[256,2048]{1,0:T(8,128)(2,1)} %x_ref.1, f32[1,2048]{1,0:T(1,128)} %bitcast.17, s32[256,2]{1,0:T(8,128)} %copy.19.ids_ref, f32[256,2]{1,0:T(8,128)} %copy.20.rw_ref, bf16[1024,256]{1,0:T(8,128)(2,1)} %multiply_convert_fusion.normed_ref, ...), custom_call_target="tpu_custom_call" | custom-call | flops 6442450944 | bytes 16777216 | tf_op jit(solution)/shard_map/pallas_call | solution.py:271
  94.2 2.3 %copy.23 = bf16[256,2048]{1,0:T(8,128)(2,1)} copy(bf16[256,2048]{1,0:T(8,128)(2,1)} %get-tuple-element.11) | data formatting | bytes 2097152
  96.5 2.3 %copy.24 = bf16[256,2048]{1,0:T(8,128)(2,1)} copy(bf16[256,2048]{1,0:T(8,128)(2,1)} %get-tuple-element.12) | data formatting | bytes 2097152
  (3 shorter events, 0.0 us)
Async XLA Ops:
  1.4 9.9 %collective-permute-start = (bf16[2,2,256]{2,1,0:T(2,128)(2,1)S(1)}, bf16[2,2,256]{2,1,0:T(2,128)(2,1)S(1)}, u32[]{:S(2)}, u32[]{:S(2)}) collective-permute-start(bf16[2,2,256]{2,1,0:T(2,128)(2,1)S(1)} %pad_maximum_fusion.1), channel_id=1, source_target_pairs={{0,4},{4,8},{8,12},{12,16},{16,20},{20,24},{24,28},{1,5},{5,9},{9,... | collective-permute-start | bytes 6152 | tf_op jit(solution)/shard_map/ppermute | solution.py:19
  11.3 2.4 %copy-start = (f32[256]{0:T(256)S(1)}, f32[256]{0:T(256)}, u32[]{:S(2)}) copy-start(f32[256]{0:T(256)} %param.17) | copy-start | bytes 3076

commit v3 on v2

--- a/solution.py
+++ b/solution.py
@@ -178,6 +178,33 @@
     many = per * n_tp * pad_slot
     back = {}
     mine = pl.ds(pl.multiple_of(me_t * pad_slot, pad_slot), pad_slot)
+    home = []
+    here = pl.ds(pl.multiple_of(me_e * rows, rows), rows)
+
+    def combine(steps):
+        for k in steps:
+            for j in range(1, n_tp):
+                back[k, j].wait_recv()
+            total = jnp.dot(
+                landed[k, :, pl.ds(width, slots)], comb[k], preferred_element_type=F32
+            ) + jnp.dot(
+                landed[k, :, pl.ds(width + slots, slots)], comb[k], preferred_element_type=F32
+            )
+            if k == 0:
+                fin[here, :] = total.astype(BF16)
+                continue
+            sums[k] = total.astype(BF16)
+            copy = pltpu.make_async_remote_copy(
+                src_ref=sums.at[k],
+                dst_ref=fin.at[here],
+                send_sem=f_send.at[k],
+                recv_sem=f_recv.at[k],
+                device_id={"ep": ep_peer(n_ep - k), "tp": me_t},
+                device_id_type=MESH,
+            )
+            copy.start()
+            home.append(copy)
+
     for c in range(chunks):
         for k in range(c * per, (c + 1) * per):
             for j in range(1, n_tp):
@@ -212,32 +239,10 @@
                 copy.start()
                 back[k, j] = copy
             comb[k, mine, :] = xin[pl.ds(k * n_tp * pad_slot, pad_slot), :]
-
-    home = []
-    here = pl.ds(pl.multiple_of(me_e * rows, rows), rows)
-    order = list(range(1, n_ep)) + [0]
-    for k in order:
-        for j in range(1, n_tp):
-            back[k, j].wait_recv()
-        total = jnp.dot(
-            landed[k, :, pl.ds(width, slots)], comb[k], preferred_element_type=F32
-        ) + jnp.dot(
-            landed[k, :, pl.ds(width + slots, slots)], comb[k], preferred_element_type=F32
-        )
-        if k == 0:
-            fin[here, :] = total.astype(BF16)
-            continue
-        sums[k] = total.astype(BF16)
-        copy = pltpu.make_async_remote_copy(
-            src_ref=sums.at[k],
-            dst_ref=fin.at[here],
-            send_sem=f_send.at[k],
-            recv_sem=f_recv.at[k],
-            device_id={"ep": ep_peer(n_ep - k), "tp": me_t},
-            device_id_type=MESH,
-        )
-        copy.start()
-        home.append(copy)
+        if c:
+            combine(range((c - 1) * per, c * per))
+
+    combine(range((chunks - 1) * per, n_ep))
     for copy in home:
         copy.wait_recv()
 
@@ -262,7 +267,7 @@
     slots = n_tp * pad_slot
     meta = round_up(3 * slots, 128)
     total = n_ep * slots
-    chunks = 2
+    chunks = 4
     part = normed.shape[0] // n_tp
     channels = mix_out_w.shape[0]
     vm = pl.BlockSpec(memory_space=pltpu.VMEM)

time: 99.3 us -> 98.8 us (level)
  no operation moved by 1% of the time
where the time goes in v3:
time: 98.8 us; the launch traced here: 98.4 us
  Pallas kernels  79.1 us (80%)
  local copies, waits for them, and re-layouts  9.85 us (10%)
  starting transfers between devices  4.87 us (5%)
  other arithmetic  3.83 us (4%)
    pallas_call x1, Pallas kernels, experts(): pl.pallas_call(functools.partial(experts_kernel, n_ep, n_tp, slot, pad_sl...  79.1 us
    unnamed x6, local copies, waits for them, and re-layouts  7.56 us
    ppermute x1, starting transfers between devices, shifted(): return lax.ppermute(value, axis, pairs)  4.87 us
  transfers between devices with their start and end apart: 1, of which 0 were waited for; matrix products, arithmetic and copies ran while one was open for 5% of the time, Pallas kernels for 0%

profile of v3, /device:TPU:0, one launch (start us, length us, event | category | flops | bytes accessed | tf_op | source)
XLA Modules:
  0.0 98.4 jit_solution(6506415443704605748)
XLA Ops:
  0.6 0.7 slice_bitcast_fusion
  1.4 4.9 %collective-permute-start = (bf16[2,2,256]{2,1,0:T(2,128)(2,1)S(1)}, bf16[2,2,256]{2,1,0:T(2,128)(2,1)S(1)}, u32[]{:S(2)}, u32[]{:S(2)}) collective-permute-start(bf16[2,2,256]{2,1,0:T(2,128)(2,1)S(1)} %pad_maximum_fusion.1), channel_id=1, source_target_pairs={{0,4},{4,8},{8,12},{12,16},{16,20},{20,24},{24,28},{1,5},{5,9},{9,... | collective-permute-start | bytes 6152 | tf_op jit(solution)/shard_map/ppermute | solution.py:19
  6.2 1.3 %convert_multiply_fusion = f32[1024,256]{1,0:T(8,128)S(1)} fusion(bf16[1024,256]{1,0:T(8,128)(2,1)} %param.15, bf16[1024,256]{1,0:T(8,128)(2,1)} %param.14), kind=kLoop, calls=%fused_computation.11 | loop fusion | flops 786432 | bytes 2097152 | tf_op jit(solution)/shard_map/mul | solution.py:342
  7.6 0.8 fusion.8
  8.4 1.5 %copy.19.ids_ref = s32[256,2]{1,0:T(8,128)} copy(s32[256,2]{0,1:T(2,128)} %param.21) | data formatting | bytes 4096 | tf_op args[8]
  9.8 1.5 %copy.20.rw_ref = f32[256,2]{1,0:T(8,128)} copy(f32[256,2]{0,1:T(2,128)} %param.22) | data formatting | bytes 4096 | tf_op args[9]
  11.3 0.0 collective-permute-done
  11.3 0.0 copy-start
  11.3 1.5 %fusion.6 = (f32[1024,256]{1,0:T(8,128)S(1)}, f32[1024,256]{1,0:T(8,128)S(1)}) fusion(f32[1024,256]{1,0:T(8,128)S(1)} %convert_multiply_fusion, f32[256]{0:T(256)S(1)} %bitcast.15, f32[2,256]{1,0:T(2,128)S(1)} %multiply_bitcast_fusion, f32[256]{0:T(256)S(1)} %bitcast.16, f32[256]{0:T(256)S(1)} %bitcast.14, bf16[1024,256]{1,0:T(8,128)(2,1)} %param.13), kind=kLoop, calls=%fused_computation.17 | loop fusion | flops 2621440 | bytes 3675136 | tf_op jit(solution)/shard_map/mul | solution.py:350
  12.8 0.3 copy.17
  13.1 0.1 bitcast_reduce_fusion
  13.2 0.1 mul.82
  13.4 0.3 copy.18
  13.7 0.0 copy-done
  13.7 0.9 multiply_convert_fusion.normed_ref
  14.6 79.1 %shard_map.140 = (bf16[256,2048]{1,0:T(8,128)(2,1)}, bf16[256,2048]{1,0:T(8,128)(2,1)}) custom-call(bf16[256,2048]{1,0:T(8,128)(2,1)} %x_ref.1, f32[1,2048]{1,0:T(1,128)} %bitcast.17, s32[256,2]{1,0:T(8,128)} %copy.19.ids_ref, f32[256,2]{1,0:T(8,128)} %copy.20.rw_ref, bf16[1024,256]{1,0:T(8,128)(2,1)} %multiply_convert_fusion.normed_ref, ...), custom_call_target="tpu_custom_call" | custom-call | flops 6442450944 | bytes 16777216 | tf_op jit(solution)/shard_map/pallas_call | solution.py:276
  93.8 2.3 %copy.23 = bf16[256,2048]{1,0:T(8,128)(2,1)} copy(bf16[256,2048]{1,0:T(8,128)(2,1)} %get-tuple-element.11) | data formatting | bytes 2097152
  96.1 2.3 %copy.24 = bf16[256,2048]{1,0:T(8,128)(2,1)} copy(bf16[256,2048]{1,0:T(8,128)(2,1)} %get-tuple-element.12) | data formatting | bytes 2097152
  (3 shorter events, 0.0 us)
Async XLA Ops:
  1.4 9.9 %collective-permute-start = (bf16[2,2,256]{2,1,0:T(2,128)(2,1)S(1)}, bf16[2,2,256]{2,1,0:T(2,128)(2,1)S(1)}, u32[]{:S(2)}, u32[]{:S(2)}) collective-permute-start(bf16[2,2,256]{2,1,0:T(2,128)(2,1)S(1)} %pad_maximum_fusion.1), channel_id=1, source_target_pairs={{0,4},{4,8},{8,12},{12,16},{16,20},{20,24},{24,28},{1,5},{5,9},{9,... | collective-permute-start | bytes 6152 | tf_op jit(solution)/shard_map/ppermute | solution.py:19
  11.3 2.4 %copy-start = (f32[256]{0:T(256)S(1)}, f32[256]{0:T(256)}, u32[]{:S(2)}) copy-start(f32[256]{0:T(256)} %param.17) | copy-start | bytes 3076
